TPU v7x, 32 devices: a whole 2x2x4 slice. The times are simulated.
32 devices in a mesh: sp: 16 (over z, y, x), tp: 2 (over core).
Axes of the slice: x: 2, y: 2, z: 4, core: 2. Of those that a mesh axis runs over, the one named last changes fastest.
Arguments:
- residual_in: bfloat16 [8192, 2048], P(('sp', 'tp')), may hold values from -6 to 6
- queries: bfloat16 [8192, 2048], P('sp', 'tp'), may hold values from -200 to 200
- keys: bfloat16 [8192, 512], P('sp', 'tp'), may hold values from -5.5 to 5.5
- values: bfloat16 [8192, 512], P('sp', 'tp'), may hold values from -6 to 6
- docs: int32 [8192], P('sp'), may hold values from 0 to 3, never falling along the last dimension, each value on 1 to 4096 neighbouring positions
- sink: float32 [32], P('tp'), may hold values from 1 to 7
- out_weight: bfloat16 [2048, 2048], P('tp'), may hold values from -0.125 to 0.125
- gate_weight: bfloat16 [2048, 5632], P('sp', 'tp'), may hold values from -0.125 to 0.125
- up_weight: bfloat16 [2048, 5632], P('sp', 'tp'), may hold values from -0.125 to 0.125
- down_weight: bfloat16 [5632, 2048], P('tp', 'sp'), may hold values from -0.078125 to 0.078125
- conv_taps: float32 [3, 5632], P(None, 'tp'), may hold values from -3.5 to 3.5
- norm_gains: float32 [3, 2048], replicated, may hold values from 0.1 to 1.9
Outputs:
- layer_out: bfloat16 [8192, 2048], P(('sp', 'tp'))
All inputs are finite; a program needn't handle non-finite values.
Results may differ from a plain program's by a relative error of at most 0.02.
Values may be sent and summed in bfloat16 or wider, within the bound.
No kernel may reach another device: no remote copies, remote signals or barrier semaphores. Data moves between devices by JAX's collectives and lax.ppermute only.
A program may use at most 128 MiB of HBM per device.

v0:
```python
import jax
import jax.numpy as jnp
from jax import lax
from jax.sharding import PartitionSpec as P

HEAD = 64
WINDOW = 128
rope_base = 10000.0
neg_large = -1e30
norm_eps = 1e-06


def padded(cells, sides, width):
    for axis, dim in sides:
        count = lax.axis_size(axis)
        ends = count - 1
        head = lax.slice_in_dim(cells, 0, width, axis=dim)
        tail = lax.slice_in_dim(cells, cells.shape[dim] - width, cells.shape[dim], axis=dim)
        cells = jnp.concatenate(
            [
                lax.ppermute(tail, axis, [(i, (i + 1) % count) for i in range(ends)]),
                cells,
                lax.ppermute(head, axis, [((i + 1) % count, i) for i in range(ends)]),
            ],
            axis=dim,
        )
    return cells


def rotate(block, positions):
    rows = block.shape[0]
    heads = block.shape[1] // HEAD
    half = HEAD // 2
    freq = rope_base ** (-jnp.arange(half, dtype=jnp.float32) * 2.0 / HEAD)
    angle = positions.astype(jnp.float32)[:, None] * freq[None, :]
    cosine = jnp.cos(angle)[:, None, :]
    sine = jnp.sin(angle)[:, None, :]
    shaped = block.astype(jnp.float32).reshape(rows, heads, 2, half)
    first = shaped[:, :, 0]
    second = shaped[:, :, 1]
    turned = jnp.stack([first * cosine - second * sine, second * cosine + first * sine], axis=2)
    return turned.reshape(rows, heads * HEAD).astype(jnp.bfloat16)


def attend(queries, keys, values, allowed, sink):
    rows = queries.shape[0]
    kv_local = keys.shape[1] // HEAD
    group = queries.shape[1] // HEAD // kv_local
    shaped_q = queries.reshape(rows, kv_local, group, HEAD)
    shaped_k = keys.reshape(keys.shape[0], kv_local, HEAD)
    shaped_v = values.reshape(values.shape[0], kv_local, HEAD)
    scores = jnp.einsum(
        "qngd,knd->ngqk", shaped_q, shaped_k, preferred_element_type=jnp.float32
    ) * HEAD ** (-0.5)
    scores = jnp.where(allowed[None, None], scores, neg_large)
    sink_group = sink.reshape(kv_local, group)[:, :, None]
    top = jnp.maximum(jnp.max(scores, axis=-1), sink_group)
    weights = jnp.exp(scores - top[..., None])
    total = jnp.sum(weights, axis=-1) + jnp.exp(sink_group - top)
    probs = (weights / total[..., None]).astype(jnp.bfloat16)
    out = jnp.einsum("ngqk,knd->qngd", probs, shaped_v, preferred_element_type=jnp.float32)
    return out.reshape(rows, kv_local * group * HEAD).astype(jnp.bfloat16)


def normalize(vector, gain):
    scale = lax.rsqrt(jnp.mean(vector * vector, axis=-1, keepdims=True) + norm_eps)
    return vector * scale * gain


def local(
    residual_in,
    queries,
    keys,
    values,
    docs,
    sink,
    out_weight,
    gate_weight,
    up_weight,
    down_weight,
    conv_taps,
    norm_gains,
):
    rows = queries.shape[0]
    offset = lax.axis_index("sp") * rows
    total_len = lax.axis_size("sp") * rows
    keys_ext, values_ext, docs_ext = (
        padded(keys, (("sp", 0),), WINDOW),
        padded(values, (("sp", 0),), WINDOW),
        padded(docs, (("sp", 0),), WINDOW),
    )
    here = offset + jnp.arange(rows, dtype=jnp.int32)
    there = offset - WINDOW + jnp.arange(rows + 2 * WINDOW, dtype=jnp.int32)
    q_rot = rotate(queries, here)
    k_rot = rotate(keys_ext, there)
    allowed = (
        (jnp.abs(there[None, :] - here[:, None]) <= WINDOW)
        & (there[None, :] >= 0)
        & (there[None, :] < total_len)
        & (docs_ext[None, :] == docs[:, None])
    )
    attended = attend(q_rot, k_rot, values_ext, allowed, sink)
    mixed = lax.psum_scatter(
        jnp.dot(attended, out_weight, preferred_element_type=jnp.float32).astype(jnp.bfloat16),
        "tp",
        scatter_dimension=0,
        tiled=True,
    ).astype(jnp.float32)
    updated = (residual_in.astype(jnp.float32) + normalize(mixed, norm_gains[0])).astype(
        jnp.bfloat16
    )
    normed = normalize(updated.astype(jnp.float32), norm_gains[1]).astype(jnp.bfloat16)
    ffn_in = lax.all_gather(normed, "tp", axis=0, tiled=True)
    gate = jnp.dot(
        ffn_in,
        lax.all_gather(gate_weight, "sp", axis=0, tiled=True),
        preferred_element_type=jnp.float32,
    )
    up = jnp.dot(
        ffn_in,
        lax.all_gather(up_weight, "sp", axis=0, tiled=True),
        preferred_element_type=jnp.float32,
    )
    gate_low = gate.astype(jnp.bfloat16)
    gate_ext = padded(gate_low, (("sp", 0),), 1).astype(jnp.float32)
    same_prev = (docs_ext[WINDOW - 1 : WINDOW - 1 + rows] == docs)[:, None]
    same_next = (docs_ext[WINDOW + 1 : WINDOW + 1 + rows] == docs)[:, None]
    conv = (
        conv_taps[0] * jnp.where(same_prev, gate_ext[:-2], 0.0)
        + conv_taps[1] * gate_ext[1:-1]
        + conv_taps[2] * jnp.where(same_next, gate_ext[2:], 0.0)
    )
    hidden = (jax.nn.silu(conv) * up).astype(jnp.bfloat16)
    terms = jnp.dot(
        hidden,
        lax.all_gather(down_weight, "sp", axis=1, tiled=True),
        preferred_element_type=jnp.float32,
    )
    ffn_out = lax.psum_scatter(
        terms.astype(jnp.bfloat16), "tp", scatter_dimension=0, tiled=True
    ).astype(jnp.float32)
    return (updated.astype(jnp.float32) + normalize(ffn_out, norm_gains[2])).astype(jnp.bfloat16)


def solution(mesh):
    in_specs = (
        P(("sp", "tp"), None),
        P("sp", "tp"),
        P("sp", "tp"),
        P("sp", "tp"),
        P("sp"),
        P("tp"),
        P("tp", None),
        P("sp", "tp"),
        P("sp", "tp"),
        P("tp", "sp"),
        P(None, "tp"),
        P(),
    )
    out_specs = P(("sp", "tp"), None)
    return jax.shard_map(local, mesh=mesh, in_specs=in_specs, out_specs=out_specs, check_vma=False)
```

profile of v0, /device:TPU:0, one launch (start us, length us, event | category | flops | bytes accessed | tf_op | source)
XLA Modules:
  0.0 611.7 jit_solution(4927613826209139854)
XLA Ops:
  6.5 1.1 copy.21
  7.7 4.9 collective-permute-start.4
  12.6 1.3 collective-permute-start.5
  13.9 0.8 fusion.38
  14.6 4.5 collective-permute-start.2
  19.2 1.3 collective-permute-start.3
  20.5 1.5 fusion.36
  22.0 4.9 collective-permute-start
  27.0 0.4 multiply_cosine_fusion
  27.4 0.3 multiply_cosine_fusion.1
  27.7 1.5 copy.24
  29.2 0.3 convert.17
  29.5 0.4 subtract_convert_fusion
  29.9 1.1 pad_maximum_fusion
  31.0 1.3 collective-permute-start.1
  32.4 1.0 fusion.23
  33.5 0.1 subtract_convert_fusion.1
  33.6 0.8 pad_maximum_fusion.2
  34.4 5.1 fusion.1
  39.6 5.3 fusion
  44.9 3.0 copy-done
  47.9 0.7 exponential_add_fusion
  48.7 0.2 copy.20
  48.8 12.0 %fusion.24 = bf16[4,64,4,512]{3,1,2,0:T(8,128)(2,1)S(1)} fusion(bf16[768,4,64,1]{0,2,3,1:T(8,128)(2,1)S(1)} %bitcast.47, f32[4,768,512,4]{2,1,3,0:T(8,128)} %copy-done, f32[4,4,512]{2,1,0:T(4,128)} %exponential_add_fusion, f32[4,4,512]{2,1,0:T(4,128)S(1)} %broadcast_maximum_fusion, pred[512,768]{0,1:T(8,128)(4,1)S(1)} %fusion.23), kind=kOutput, calls=%fused_computation.42 | convolution fusion | flops 837287936 | bytes 27066368 | tf_op jit(solution)/shard_map/ngqk,knd->qngd/dot_general | solution.py:61
  60.9 3.8 convolution_convert_fusion.1
  64.8 15.3 %reduce-scatter.3.cloned.1.call-done = bf16[256,2048]{1,0:T(8,128)(2,1)} async-done(((bf16[512,2048]{1,0:T(8,128)(2,1)}), bf16[256,2048]{1,0:T(8,128)(2,1)}) %reduce-scatter.3.cloned.1.call-update) | async-done | bytes 1048592 | tf_op jit(solution)/shard_map/reduce_scatter | solution.py:103
  80.1 1.5 fusion.11
  81.7 1.9 fusion.17
  83.6 1.3 fusion.19
  84.9 0.7 all-gather.7.cloned.1.call-update
  85.7 0.5 all-gather.11.cloned.1.call-update
  86.2 0.5 all-gather.9.cloned.1.call-update
  86.8 0.2 reduce-scatter.5.cloned.1.call-start
  87.0 0.1 slice_reduce_fusion.2
  87.1 9.8 %all-gather.5.cloned.1.call-done = bf16[512,2048]{1,0:T(8,128)(2,1)} async-done(((bf16[256,2048]{1,0:T(8,128)(2,1)}), bf16[512,2048]{1,0:T(8,128)(2,1)}) %all-gather.5.cloned.1.call-update) | async-done | bytes 2097168 | tf_op jit(solution)/shard_map/all_gather | solution.py:113
  96.9 145.4 %all-gather.7.cloned.1.call-done = bf16[2048,2816]{1,0:T(8,128)(2,1)} async-done(((bf16[128,2816]{1,0:T(8,128)(2,1)}), bf16[2048,2816]{1,0:T(8,128)(2,1)}) %all-gather.7.cloned.1.call-update) | async-done | bytes 11534352 | tf_op jit(solution)/shard_map/all_gather | solution.py:116
  242.3 10.9 %convolution_convert_fusion = bf16[512,2816]{1,0:T(8,128)(2,1)S(1)} fusion(bf16[512,2048]{1,0:T(8,128)(2,1)} %all-gather.5.cloned.1.call-done, bf16[2048,2816]{1,0:T(8,128)(2,1)} %all-gather.7.cloned.1.call-done), kind=kOutput, calls=%fused_computation.14 | convolution fusion | flops 5907021824 | bytes 16515072 | tf_op jit(solution)/shard_map/dot_general | solution.py:114
  253.3 3.2 collective-permute-start.6
  256.4 1.3 collective-permute-start.7
  257.8 0.2 collective-permute-done.6
  258.0 4.4 collective-permute-done.7
  262.4 3.1 maximum_convert_fusion
  265.5 159.9 %all-gather.11.cloned.1.call-done = bf16[2816,2048]{1,0:T(8,128)(2,1)} async-done(((bf16[2816,128]{1,0:T(8,128)(2,1)}), bf16[2816,2048]{1,0:T(8,128)(2,1)}) %all-gather.11.cloned.1.call-update) | async-done | bytes 11534352 | tf_op jit(solution)/shard_map/all_gather | solution.py:136
  425.3 142.2 %all-gather.9.cloned.1.call-done = bf16[2048,2816]{1,0:T(8,128)(2,1)} async-done(((bf16[128,2816]{1,0:T(8,128)(2,1)}), bf16[2048,2816]{1,0:T(8,128)(2,1)}) %all-gather.9.cloned.1.call-update) | async-done | bytes 11534352 | tf_op jit(solution)/shard_map/all_gather | solution.py:121
  567.6 25.0 %convolution_convert_fusion.2 = bf16[512,2048]{1,0:T(8,128)(2,1)} fusion(bf16[2816,2048]{1,0:T(8,128)(2,1)} %all-gather.11.cloned.1.call-done, f32[514,2816]{1,0:T(8,128)} %maximum_convert_fusion, f32[2816]{0:T(1024)S(1)} %get-tuple-element.6, f32[2816]{0:T(1024)S(1)} %get-tuple-element.7, f32[2816]{0:T(1024)S(1)} %get-tuple-element.5, ...), kind=kOutput, calls=%fused_computation.19 | convolution fusion | flops 11830951936 | bytes 44599296 | tf_op jit(solution)/shard_map/dot_general | solution.py:134
  592.6 8.1 %reduce-scatter.5.cloned.1.call-done = bf16[256,2048]{1,0:T(8,128)(2,1)} async-done(((bf16[512,2048]{1,0:T(8,128)(2,1)}), bf16[256,2048]{1,0:T(8,128)(2,1)}) %reduce-scatter.5.cloned.1.call-update) | async-done | bytes 1048592 | tf_op jit(solution)/shard_map/reduce_scatter | solution.py:139
  600.7 1.5 fusion.15
  602.2 2.6 fusion.20
  (48 shorter events, 0.7 us)
Async XLA Ops:
  6.5 73.6 %reduce-scatter.3.cloned.1.call-start = ((), (), s32[]{:S(2)}) async-start(), calls=%async_computation.2 | async-start | bytes 3145728 | tf_op jit(solution)/shard_map/reduce_scatter | solution.py:103
  7.6 23.3 %copy-start.6 = (f32[16]{0:T(128)S(1)}, f32[16]{0:T(128)}, u32[]{:S(2)}) copy-start(f32[16]{0:T(128)} %param.17) | copy-start | bytes 196
  7.6 24.7 %copy-start.3 = (s32[512]{0:T(512)S(1)}, s32[512]{0:T(512)}, u32[]{:S(2)}) copy-start(s32[512]{0:T(512)} %param.16) | copy-start | bytes 6148
  7.7 25.7 %collective-permute-start.4 = (bf16[128,256]{0,1:T(8,128)(2,1)S(1)}, bf16[128,256]{0,1:T(8,128)(2,1)S(1)}, u32[]{:S(2)}, u32[]{:S(2)}) collective-permute-start(bf16[128,256]{0,1:T(8,128)(2,1)S(1)} %get-tuple-element.16), channel_id=1, source_target_pairs={{0,2},{2,4},{4,6},{6,8},{8,10},{10,12},{12,14},{14,16},{16,18},{18... | collective-permute-start | bytes 196616 | tf_op jit(solution)/shard_map/ppermute | solution.py:21
  12.6 20.9 %collective-permute-start.5 = (bf16[128,256]{0,1:T(8,128)(2,1)S(1)}, bf16[128,256]{0,1:T(8,128)(2,1)S(1)}, u32[]{:S(2)}, u32[]{:S(2)}) collective-permute-start(bf16[128,256]{0,1:T(8,128)(2,1)S(1)} %get-tuple-element.17), channel_id=1, source_target_pairs={{2,0},{4,2},{6,4},{8,6},{10,8},{12,10},{14,12},{16,14},{18,16},{20... | collective-permute-start | bytes 196616 | tf_op jit(solution)/shard_map/ppermute | solution.py:23
  14.6 16.4 %collective-permute-start.2 = (s32[128]{0:T(128)S(1)}, s32[128]{0:T(128)S(1)}, u32[]{:S(2)}, u32[]{:S(2)}) collective-permute-start(s32[128]{0:T(128)S(1)} %get-tuple-element.31), channel_id=1, source_target_pairs={{0,2},{2,4},{4,6},{6,8},{8,10},{10,12},{12,14},{14,16},{16,18},{18... | collective-permute-start | bytes 1544 | tf_op jit(solution)/shard_map/ppermute | solution.py:21
  19.2 13.2 %collective-permute-start.3 = (s32[128]{0:T(128)S(1)}, s32[128]{0:T(128)S(1)}, u32[]{:S(2)}, u32[]{:S(2)}) collective-permute-start(s32[128]{0:T(128)S(1)} %get-tuple-element.32), channel_id=1, source_target_pairs={{2,0},{4,2},{6,4},{8,6},{10,8},{12,10},{14,12},{16,14},{18,16},{20... | collective-permute-start | bytes 1544 | tf_op jit(solution)/shard_map/ppermute | solution.py:23
  22.0 26.6 %collective-permute-start = (bf16[128,256]{1,0:T(8,128)(2,1)}, bf16[128,256]{1,0:T(8,128)(2,1)S(1)}, u32[]{:S(2)}, u32[]{:S(2)}) collective-permute-start(bf16[128,256]{1,0:T(8,128)(2,1)} %get-tuple-element.18), channel_id=1, source_target_pairs={{0,2},{2,4},{4,6},{6,8},{8,10},{10,12},{12,14},{14,16},{16,18},{18... | collective-permute-start | bytes 196616 | tf_op jit(solution)/shard_map/ppermute | solution.py:21
  31.0 17.6 %collective-permute-start.1 = (bf16[128,256]{1,0:T(8,128)(2,1)}, bf16[128,256]{1,0:T(8,128)(2,1)S(1)}, u32[]{:S(2)}, u32[]{:S(2)}) collective-permute-start(bf16[128,256]{1,0:T(8,128)(2,1)} %get-tuple-element.19), channel_id=1, source_target_pairs={{2,0},{4,2},{6,4},{8,6},{10,8},{12,10},{14,12},{16,14},{18,16},{20... | collective-permute-start | bytes 196616 | tf_op jit(solution)/shard_map/ppermute | solution.py:23
  39.5 8.4 %copy-start = (f32[4,768,512,4]{2,1,3,0:T(8,128)}, f32[4,768,512,4]{2,1,3,0:T(8,128)S(1)}, u32[]{:S(2)}) copy-start(f32[4,768,512,4]{2,1,3,0:T(8,128)S(1)} %get-tuple-element.34) | copy-start | bytes 75497472
  39.6 9.0 %copy-start.2 = (bf16[512,256]{1,0:T(8,128)(2,1)S(1)}, bf16[512,256]{1,0:T(8,128)(2,1)}, u32[]{:S(2)}) copy-start(bf16[512,256]{1,0:T(8,128)(2,1)} %param.15) | copy-start | bytes 786436
  48.8 12.0 %copy-start.7 = (bf16[1024,2048]{1,0:T(8,128)(2,1)S(1)}, bf16[1024,2048]{1,0:T(8,128)(2,1)}, u32[]{:S(2)}) copy-start(bf16[1024,2048]{1,0:T(8,128)(2,1)} %param.18) | copy-start | bytes 12582916
  60.9 3.9 copy-start.5
  60.9 20.8 %copy-start.1 = (bf16[256,2048]{1,0:T(8,128)(2,1)S(1)}, bf16[256,2048]{1,0:T(8,128)(2,1)}, u32[]{:S(2)}) copy-start(bf16[256,2048]{1,0:T(8,128)(2,1)} %param.12) | copy-start | bytes 3145732
  64.7 22.3 %copy-start.4 = (f32[3,2816]{1,0:T(4,128)S(1)}, f32[3,2816]{1,0:T(4,128)}, u32[]{:S(2)}) copy-start(f32[3,2816]{1,0:T(4,128)} %param.22) | copy-start | bytes 101380
  64.7 32.2 %all-gather.5.cloned.1.call-start = ((), (), s32[]{:S(2)}) async-start(), calls=%async_computation.3 | async-start | bytes 3145728 | tf_op jit(solution)/shard_map/all_gather | solution.py:113
  84.9 157.4 %all-gather.7.cloned.1.call-start = ((), (), s32[]{:S(2)}) async-start(), calls=%async_computation.4 | async-start | bytes 12255232 | tf_op jit(solution)/shard_map/all_gather | solution.py:116
  85.6 339.7 %all-gather.11.cloned.1.call-start = ((), (), s32[]{:S(2)}) async-start(), calls=%async_computation.6 | async-start | bytes 12255232 | tf_op jit(solution)/shard_map/all_gather | solution.py:136
  86.2 481.4 %all-gather.9.cloned.1.call-start = ((), (), s32[]{:S(2)}) async-start(), calls=%async_computation.5 | async-start | bytes 12255232 | tf_op jit(solution)/shard_map/all_gather | solution.py:121
  86.8 513.9 %reduce-scatter.5.cloned.1.call-start = ((), (), s32[]{:S(2)}) async-start(), calls=%async_computation.7 | async-start | bytes 3145728 | tf_op jit(solution)/shard_map/reduce_scatter | solution.py:139
  253.3 4.7 collective-permute-start.6
  256.4 5.9 collective-permute-start.7
Sparse Core Ops, SparseCore 0:
  64.8 15.2 reduce-scatter.2
  85.0 11.8 all-gather.4
  99.7 142.5 all-gather.6
  244.8 180.4 all-gather.10
  427.9 139.5 all-gather.8
  592.7 7.9 reduce-scatter.4
where the time goes:
time: 612 us
  waiting for transfers between devices  487 us (80%)
  matrix products  56.8 us (9%)
  starting transfers between devices  23 us (4%)
  other arithmetic  22.6 us (4%)
  between operations  13.9 us (2%)
  local copies, waits for them, and re-layouts  8.33 us (1%)
    all_gather x1, waiting for transfers between devices, local(): lax.all_gather(down_weight, 'sp', axis=1, tiled=True)  160 us
    all_gather x1, waiting for transfers between devices, local(): lax.all_gather(gate_weight, 'sp', axis=0, tiled=True)  145 us
    all_gather x1, waiting for transfers between devices, local(): lax.all_gather(up_weight, 'sp', axis=0, tiled=True)  142 us
    dot_general x1, matrix products, local(): jnp.dot(hidden, lax.all_gather(down_weight, 'sp', axis=1, tiled=True), pr...  25 us
    ppermute x4, starting transfers between devices, padded(): lax.ppermute(tail, axis, [(i, (i + 1) % count) for i in range(ends)])  17.5 us
    reduce_scatter x1, waiting for transfers between devices, local(): lax.psum_scatter(jnp.dot(attended, out_weight, preferred_element_type=jnp...  15.3 us
  transfers between devices with their start and end apart: 14, of which 8 were waited for; matrix products, arithmetic and copies ran while one was open for 6% of the time, Pallas kernels for 0%

commit v1 on v0

--- a/solution.py
+++ b/solution.py
@@ -133,7 +133,7 @@
     hidden = (jax.nn.silu(conv) * up).astype(jnp.bfloat16)
     terms = jnp.dot(
         hidden,
-        lax.all_gather(down_weight, "sp", axis=1, tiled=True),
+        jnp.concatenate(lax.all_gather(down_weight, "sp"), axis=1),
         preferred_element_type=jnp.float32,
     )
     ffn_out = lax.psum_scatter(

time: 612 us -> 571 us (0.933)
  waiting for transfers between devices: 487 us -> 428 us
  local copies, waits for them, and re-layouts: 8.33 us -> 25.2 us
    all_gather x1, waiting for transfers between devices: 160 us -> 125 us  [local(): lax.all_gather(down_weight, 'sp')]
    all_gather x1, waiting for transfers between devices: 142 us -> 122 us  [local(): lax.all_gather(up_weight, 'sp', axis=0, tiled=True)]
    reshape x0 -> x1, local copies, waits for them, and re-layouts: none -> 15.2 us  [local(): jnp.concatenate(lax.all_gather(down_weight, 'sp'), axis=1)]
  transfers between devices with their start and end apart: 14 -> 14, of which waited for: 8 -> 6; matrix products, arithmetic and copies ran while one was open for 6% -> 9% of each run, Pallas kernels for 0% -> 0%
where the time goes in v1:
time: 571 us; the launch traced here: 570 us
  waiting for transfers between devices  428 us (75%)
  matrix products  56.2 us (10%)
  local copies, waits for them, and re-layouts  25.2 us (4%)
  other arithmetic  24.4 us (4%)
  starting transfers between devices  23 us (4%)
  between operations  13.9 us (2%)
    all_gather x1, waiting for transfers between devices, local(): lax.all_gather(gate_weight, 'sp', axis=0, tiled=True)  145 us
    all_gather x1, waiting for transfers between devices, local(): lax.all_gather(down_weight, 'sp')  125 us
    all_gather x1, waiting for transfers between devices, local(): lax.all_gather(up_weight, 'sp', axis=0, tiled=True)  122 us
    dot_general x1, matrix products, local(): jnp.dot(hidden, jnp.concatenate(lax.all_gather(down_weight, 'sp'), axis=1...  24.3 us
    ppermute x4, starting transfers between devices, padded(): lax.ppermute(tail, axis, [(i, (i + 1) % count) for i in range(ends)])  17.5 us
    reduce_scatter x1, waiting for transfers between devices, local(): lax.psum_scatter(jnp.dot(attended, out_weight, preferred_element_type=jnp...  15.3 us
    reshape x1, local copies, waits for them, and re-layouts, local(): jnp.concatenate(lax.all_gather(down_weight, 'sp'), axis=1)  15.2 us
    dot_general x1, matrix products, attend(): jnp.einsum('ngqk,knd->qngd', probs, shaped_v, preferred_element_type=jnp....  12 us
  transfers between devices with their start and end apart: 14, of which 6 were waited for; matrix products, arithmetic and copies ran while one was open for 9% of the time, Pallas kernels for 0%

profile of v1, /device:TPU:0, one launch (start us, length us, event | category | flops | bytes accessed | tf_op | source)
XLA Modules:
  0.0 570.5 jit_solution(5342564187769399239)
XLA Ops:
  6.5 1.1 copy.27
  7.7 4.9 collective-permute-start.4
  12.6 1.3 collective-permute-start.5
  13.9 0.8 fusion.38
  14.6 4.5 collective-permute-start.2
  19.2 1.3 collective-permute-start.3
  20.5 1.5 fusion.36
  22.0 4.9 collective-permute-start
  27.0 0.4 multiply_cosine_fusion
  27.4 0.3 multiply_cosine_fusion.1
  27.7 1.5 copy.30
  29.2 0.3 convert.17
  29.5 0.4 subtract_convert_fusion
  29.9 1.1 pad_maximum_fusion
  31.1 1.3 collective-permute-start.1
  32.4 1.0 fusion.23
  33.5 0.1 subtract_convert_fusion.1
  33.6 0.8 pad_maximum_fusion.2
  34.4 5.1 fusion.1
  39.6 5.3 fusion
  44.9 3.0 copy-done
  47.9 0.7 exponential_add_fusion
  48.7 0.2 copy.26
  48.9 12.0 %fusion.24 = bf16[4,64,4,512]{3,1,2,0:T(8,128)(2,1)S(1)} fusion(bf16[768,4,64,1]{0,2,3,1:T(8,128)(2,1)S(1)} %bitcast.53, f32[4,768,512,4]{2,1,3,0:T(8,128)} %copy-done, f32[4,4,512]{2,1,0:T(4,128)} %exponential_add_fusion, f32[4,4,512]{2,1,0:T(4,128)S(1)} %broadcast_maximum_fusion, pred[512,768]{0,1:T(8,128)(4,1)S(1)} %fusion.23), kind=kOutput, calls=%fused_computation.42 | convolution fusion | flops 837287936 | bytes 27066368 | tf_op jit(solution)/shard_map/ngqk,knd->qngd/dot_general | solution.py:61
  60.9 3.8 convolution_convert_fusion.1
  64.8 15.3 %reduce-scatter.3.cloned.1.call-done = bf16[256,2048]{1,0:T(8,128)(2,1)} async-done(((bf16[512,2048]{1,0:T(8,128)(2,1)}), bf16[256,2048]{1,0:T(8,128)(2,1)}) %reduce-scatter.3.cloned.1.call-update) | async-done | bytes 1048592 | tf_op jit(solution)/shard_map/reduce_scatter | solution.py:103
  80.2 1.5 fusion.11
  81.7 1.9 fusion.17
  83.6 1.3 fusion.19
  84.9 0.7 all-gather.8.cloned.1.call-update
  85.7 0.5 all-gather.12.cloned.1.call-update
  86.2 0.5 all-gather.10.cloned.1.call-update
  86.8 0.2 reduce-scatter.5.cloned.1.call-start
  87.0 0.1 slice_reduce_fusion.2
  87.1 9.8 %all-gather.6.cloned.1.call-done = bf16[512,2048]{1,0:T(8,128)(2,1)} async-done(((bf16[256,2048]{1,0:T(8,128)(2,1)}), bf16[512,2048]{1,0:T(8,128)(2,1)}) %all-gather.6.cloned.1.call-update) | async-done | bytes 2097168 | tf_op jit(solution)/shard_map/all_gather | solution.py:113
  96.9 145.4 %all-gather.8.cloned.1.call-done = bf16[2048,2816]{1,0:T(8,128)(2,1)} async-done(((bf16[128,2816]{1,0:T(8,128)(2,1)}), bf16[2048,2816]{1,0:T(8,128)(2,1)}) %all-gather.8.cloned.1.call-update) | async-done | bytes 11534352 | tf_op jit(solution)/shard_map/all_gather | solution.py:116
  242.3 10.9 %convolution_convert_fusion = bf16[512,2816]{1,0:T(8,128)(2,1)S(1)} fusion(bf16[512,2048]{1,0:T(8,128)(2,1)} %all-gather.6.cloned.1.call-done, bf16[2048,2816]{1,0:T(8,128)(2,1)} %all-gather.8.cloned.1.call-done), kind=kOutput, calls=%fused_computation.14 | convolution fusion | flops 5907021824 | bytes 16515072 | tf_op jit(solution)/shard_map/dot_general | solution.py:114
  253.3 1.6 copy-done.1
  254.9 3.2 collective-permute-start.6
  258.1 1.3 collective-permute-start.7
  259.5 125.3 %all-gather.12.cloned.1.call-done = bf16[45056,128]{1,0:T(8,128)(2,1)} async-done(((bf16[2816,128]{1,0:T(8,128)(2,1)}), bf16[45056,128]{1,0:T(8,128)(2,1)}) %all-gather.12.cloned.1.call-update) | async-done | bytes 11534352 | tf_op jit(solution)/shard_map/all_gather | solution.py:136
  384.8 15.2 %copy.32 = bf16[2816,16,128]{0,2,1:T(8,128)(2,1)} copy(bf16[2816,16,128]{2,0,1:T(8,128)(2,1)} %bitcast.47) | data formatting | bytes 23068672 | tf_op jit(solution)/shard_map/reshape | solution.py:136
  400.0 5.0 maximum_convert_fusion
  404.9 122.1 %all-gather.10.cloned.1.call-done = bf16[2048,2816]{1,0:T(8,128)(2,1)} async-done(((bf16[128,2816]{1,0:T(8,128)(2,1)}), bf16[2048,2816]{1,0:T(8,128)(2,1)}) %all-gather.10.cloned.1.call-update) | async-done | bytes 11534352 | tf_op jit(solution)/shard_map/all_gather | solution.py:121
  527.0 24.3 %convolution_convert_fusion.2 = bf16[512,2048]{1,0:T(8,128)(2,1)} fusion(bf16[2816,2048]{0,1:T(8,128)(2,1)} %bitcast.48, f32[514,2816]{1,0:T(8,128)} %maximum_convert_fusion, f32[2816]{0:T(1024)S(1)} %get-tuple-element.6, f32[2816]{0:T(1024)S(1)} %get-tuple-element.7, f32[2816]{0:T(1024)S(1)} %get-tuple-element.5, pred[512]{0:T(512)(128)(4,1)S(1)} %get-tuple-element.28, ...), kind=kOutput, calls=%fused_computation.19 | convolution fusion | flops 11830951936 | bytes 44599296 | tf_op jit(solution)/shard_map/dot_general | solution.py:134
  551.4 8.1 %reduce-scatter.5.cloned.1.call-done = bf16[256,2048]{1,0:T(8,128)(2,1)} async-done(((bf16[512,2048]{1,0:T(8,128)(2,1)}), bf16[256,2048]{1,0:T(8,128)(2,1)}) %reduce-scatter.5.cloned.1.call-update) | async-done | bytes 1048592 | tf_op jit(solution)/shard_map/reduce_scatter | solution.py:139
  559.4 1.5 fusion.15
  561.0 2.6 fusion.20
  (51 shorter events, 0.7 us)
Async XLA Ops:
  6.5 73.6 %reduce-scatter.3.cloned.1.call-start = ((), (), s32[]{:S(2)}) async-start(), calls=%async_computation.2 | async-start | bytes 3145728 | tf_op jit(solution)/shard_map/reduce_scatter | solution.py:103
  7.6 23.3 %copy-start.7 = (f32[16]{0:T(128)S(1)}, f32[16]{0:T(128)}, u32[]{:S(2)}) copy-start(f32[16]{0:T(128)} %param.17) | copy-start | bytes 196
  7.6 24.7 %copy-start.4 = (s32[512]{0:T(512)S(1)}, s32[512]{0:T(512)}, u32[]{:S(2)}) copy-start(s32[512]{0:T(512)} %param.16) | copy-start | bytes 6148
  7.7 25.7 %collective-permute-start.4 = (bf16[128,256]{0,1:T(8,128)(2,1)S(1)}, bf16[128,256]{0,1:T(8,128)(2,1)S(1)}, u32[]{:S(2)}, u32[]{:S(2)}) collective-permute-start(bf16[128,256]{0,1:T(8,128)(2,1)S(1)} %get-tuple-element.16), channel_id=1, source_target_pairs={{0,2},{2,4},{4,6},{6,8},{8,10},{10,12},{12,14},{14,16},{16,18},{18... | collective-permute-start | bytes 196616 | tf_op jit(solution)/shard_map/ppermute | solution.py:21
  12.6 20.9 %collective-permute-start.5 = (bf16[128,256]{0,1:T(8,128)(2,1)S(1)}, bf16[128,256]{0,1:T(8,128)(2,1)S(1)}, u32[]{:S(2)}, u32[]{:S(2)}) collective-permute-start(bf16[128,256]{0,1:T(8,128)(2,1)S(1)} %get-tuple-element.17), channel_id=1, source_target_pairs={{2,0},{4,2},{6,4},{8,6},{10,8},{12,10},{14,12},{16,14},{18,16},{20... | collective-permute-start | bytes 196616 | tf_op jit(solution)/shard_map/ppermute | solution.py:23
  14.6 16.4 %collective-permute-start.2 = (s32[128]{0:T(128)S(1)}, s32[128]{0:T(128)S(1)}, u32[]{:S(2)}, u32[]{:S(2)}) collective-permute-start(s32[128]{0:T(128)S(1)} %get-tuple-element.31), channel_id=1, source_target_pairs={{0,2},{2,4},{4,6},{6,8},{8,10},{10,12},{12,14},{14,16},{16,18},{18... | collective-permute-start | bytes 1544 | tf_op jit(solution)/shard_map/ppermute | solution.py:21
  19.2 13.2 %collective-permute-start.3 = (s32[128]{0:T(128)S(1)}, s32[128]{0:T(128)S(1)}, u32[]{:S(2)}, u32[]{:S(2)}) collective-permute-start(s32[128]{0:T(128)S(1)} %get-tuple-element.32), channel_id=1, source_target_pairs={{2,0},{4,2},{6,4},{8,6},{10,8},{12,10},{14,12},{16,14},{18,16},{20... | collective-permute-start | bytes 1544 | tf_op jit(solution)/shard_map/ppermute | solution.py:23
  22.0 26.6 %collective-permute-start = (bf16[128,256]{1,0:T(8,128)(2,1)}, bf16[128,256]{1,0:T(8,128)(2,1)S(1)}, u32[]{:S(2)}, u32[]{:S(2)}) collective-permute-start(bf16[128,256]{1,0:T(8,128)(2,1)} %get-tuple-element.18), channel_id=1, source_target_pairs={{0,2},{2,4},{4,6},{6,8},{8,10},{10,12},{12,14},{14,16},{16,18},{18... | collective-permute-start | bytes 196616 | tf_op jit(solution)/shard_map/ppermute | solution.py:21
  31.1 17.6 %collective-permute-start.1 = (bf16[128,256]{1,0:T(8,128)(2,1)}, bf16[128,256]{1,0:T(8,128)(2,1)S(1)}, u32[]{:S(2)}, u32[]{:S(2)}) collective-permute-start(bf16[128,256]{1,0:T(8,128)(2,1)} %get-tuple-element.19), channel_id=1, source_target_pairs={{2,0},{4,2},{6,4},{8,6},{10,8},{12,10},{14,12},{16,14},{18,16},{20... | collective-permute-start | bytes 196616 | tf_op jit(solution)/shard_map/ppermute | solution.py:23
  39.5 8.4 %copy-start = (f32[4,768,512,4]{2,1,3,0:T(8,128)}, f32[4,768,512,4]{2,1,3,0:T(8,128)S(1)}, u32[]{:S(2)}) copy-start(f32[4,768,512,4]{2,1,3,0:T(8,128)S(1)} %get-tuple-element.34) | copy-start | bytes 75497472
  39.6 9.0 %copy-start.3 = (bf16[512,256]{1,0:T(8,128)(2,1)S(1)}, bf16[512,256]{1,0:T(8,128)(2,1)}, u32[]{:S(2)}) copy-start(bf16[512,256]{1,0:T(8,128)(2,1)} %param.15) | copy-start | bytes 786436
  48.9 12.0 %copy-start.8 = (bf16[1024,2048]{1,0:T(8,128)(2,1)S(1)}, bf16[1024,2048]{1,0:T(8,128)(2,1)}, u32[]{:S(2)}) copy-start(bf16[1024,2048]{1,0:T(8,128)(2,1)} %param.18) | copy-start | bytes 12582916
  60.9 3.9 copy-start.6
  60.9 20.8 %copy-start.2 = (bf16[256,2048]{1,0:T(8,128)(2,1)S(1)}, bf16[256,2048]{1,0:T(8,128)(2,1)}, u32[]{:S(2)}) copy-start(bf16[256,2048]{1,0:T(8,128)(2,1)} %param.12) | copy-start | bytes 3145732
  64.7 22.3 %copy-start.5 = (f32[3,2816]{1,0:T(4,128)S(1)}, f32[3,2816]{1,0:T(4,128)}, u32[]{:S(2)}) copy-start(f32[3,2816]{1,0:T(4,128)} %param.22) | copy-start | bytes 101380
  64.7 32.2 %all-gather.6.cloned.1.call-start = ((), (), s32[]{:S(2)}) async-start(), calls=%async_computation.3 | async-start | bytes 3145728 | tf_op jit(solution)/shard_map/all_gather | solution.py:113
  84.9 157.4 %all-gather.8.cloned.1.call-start = ((), (), s32[]{:S(2)}) async-start(), calls=%async_computation.4 | async-start | bytes 12255232 | tf_op jit(solution)/shard_map/all_gather | solution.py:116
  85.6 299.2 %all-gather.12.cloned.1.call-start = ((), (), s32[]{:S(2)}) async-start(), calls=%async_computation.7 | async-start | bytes 12255232 | tf_op jit(solution)/shard_map/all_gather | solution.py:136
  86.2 440.8 %all-gather.10.cloned.1.call-start = ((), (), s32[]{:S(2)}) async-start(), calls=%async_computation.5 | async-start | bytes 12255232 | tf_op jit(solution)/shard_map/all_gather | solution.py:121
  86.8 472.7 %reduce-scatter.5.cloned.1.call-start = ((), (), s32[]{:S(2)}) async-start(), calls=%async_computation.6 | async-start | bytes 3145728 | tf_op jit(solution)/shard_map/reduce_scatter | solution.py:139
  253.2 1.6 copy-start.1
  254.9 145.1 %collective-permute-start.6 = (bf16[1,2816]{1,0:T(2,128)(2,1)S(1)}, bf16[1,2816]{1,0:T(2,128)(2,1)S(1)}, u32[]{:S(2)}, u32[]{:S(2)}) collective-permute-start(bf16[1,2816]{1,0:T(2,128)(2,1)S(1)} %get-tuple-element.10), channel_id=1, source_target_pairs={{0,2},{2,4},{4,6},{6,8},{8,10},{10,12},{12,14},{14,16},{16,18},{18... | collective-permute-start | bytes 16904 | tf_op jit(solution)/shard_map/ppermute | solution.py:21
  258.1 141.9 %collective-permute-start.7 = (bf16[1,2816]{1,0:T(2,128)(2,1)S(1)}, bf16[1,2816]{1,0:T(2,128)(2,1)S(1)}, u32[]{:S(2)}, u32[]{:S(2)}) collective-permute-start(bf16[1,2816]{1,0:T(2,128)(2,1)S(1)} %get-tuple-element.11), channel_id=1, source_target_pairs={{2,0},{4,2},{6,4},{8,6},{10,8},{12,10},{14,12},{16,14},{18,16},{20... | collective-permute-start | bytes 16904 | tf_op jit(solution)/shard_map/ppermute | solution.py:23
Sparse Core Ops, SparseCore 0:
  64.8 15.2 reduce-scatter.2
  85.0 11.8 all-gather.5
  99.7 142.5 all-gather.7
  244.9 139.8 all-gather.11
  387.4 139.5 all-gather.9
  551.5 7.9 reduce-scatter.4
